TPU v7x, 32 devices: a whole 2x2x4 slice. The times are simulated.
32 devices in a mesh: sp: 8 (over z, y), tp: 4 (over x, core).
Axes of the slice: x: 2, y: 2, z: 4, core: 2. Of those that a mesh axis runs over, the one named last changes fastest.
Arguments:
- tokens: bfloat16 [3072, 2048], P('sp', 'tp'), may hold values from -16 to 16
- norm_gain: bfloat16 [2048], replicated, may hold values from 0.099609375 to 1.8984375
- w_query: bfloat16 [2048, 1024], P(None, 'tp'), may hold values from -0.125 to 0.125
- w_key: bfloat16 [2048, 1024], P(None, 'tp'), may hold values from -0.125 to 0.125
- w_value: bfloat16 [2048, 1024], P(None, 'tp'), may hold values from -0.125 to 0.125
- key_bias: bfloat16 [8, 3072], P('tp', 'sp'), may hold values from -13 to 0
- w_glu_value: bfloat16 [2048, 1024], P(None, 'tp'), may hold values from -0.125 to 0.125
- w_glu_gate: bfloat16 [2048, 1024], P(None, 'tp'), may hold values from -0.125 to 0.125
- conv_weight: bfloat16 [31, 1024], replicated, may hold values from -4 to 4
- conv_bias: bfloat16 [1024], replicated, may hold values from 0 to 16
- ln_gain: bfloat16 [1024], replicated, may hold values from 0.099609375 to 1.8984375
- w_out_att: bfloat16 [1024, 2048], replicated, may hold values from -0.75 to 0.75
- w_out_conv: bfloat16 [1024, 2048], replicated, may hold values from -0.1875 to 0.1875
Outputs:
- mixed: bfloat16 [3072, 2048], P(('sp', 'tp'))
- weight_log: float32 [8, 3072], P('tp', 'sp')
All inputs are finite; a program needn't handle non-finite values.
Results may differ from a plain program's by a relative error of at most 0.007.
Values may be sent and summed in bfloat16 or wider, within the bound.
A program may use at most 192 MiB of HBM per device.

v0:
```python
import jax
import jax.numpy as jnp
from jax import lax
from jax.sharding import PartitionSpec as P

D = 2048
HEAD = 128
CF_WIDTH = 1024
epsilon = 1e-06


def from_behind(block, axis, distance):
    devices = range(lax.axis_size(axis))
    route = [(i - distance, i) for i in devices if i - distance in devices]
    return lax.ppermute(block, axis, route)


def rounded(values):
    return lax.optimization_barrier(values.astype(jnp.bfloat16)).astype(jnp.float32)


def later_matrix(count):
    row_ids = lax.broadcasted_iota(jnp.int32, (count, count), 0)
    col_ids = lax.broadcasted_iota(jnp.int32, (count, count), 1)
    return (row_ids > col_ids).astype(jnp.float32)


def block_terms(query_matrix_rows, key_rows, value_rows, bias_rows):
    head_size = query_matrix_rows.shape[-1]
    scores = jnp.einsum(
        "qhe,khe->hqk", query_matrix_rows, key_rows, preferred_element_type=jnp.float32
    )
    scores = scores * head_size ** (-0.5) + bias_rows.astype(jnp.float32)[:, None, :]
    keep_log = jax.nn.log_sigmoid(-scores)
    row_ids = lax.broadcasted_iota(jnp.int32, scores.shape, 1)
    col_ids = lax.broadcasted_iota(jnp.int32, scores.shape, 2)
    allowed = col_ids <= row_ids
    keep_log = jnp.where(allowed, keep_log, 0.0)
    later_sum = jnp.einsum(
        "hqj,jk->hqk", keep_log, later_matrix(scores.shape[2]), precision=lax.Precision.HIGHEST
    )
    weights = jnp.exp(jax.nn.log_sigmoid(scores) + later_sum)
    weights = jnp.where(allowed, weights, 0.0)
    block_out = jnp.einsum(
        "hqk,khe->qhe", weights.astype(jnp.bfloat16), value_rows, preferred_element_type=jnp.float32
    )
    return (block_out, jnp.sum(keep_log, axis=2))


def window_terms(query_matrix_rows, key_window, value_window, bias_window, valid_count):
    tok_rows, heads_here, head_size = query_matrix_rows.shape
    block_count = key_window.shape[0] // tok_rows
    key_blocks = key_window.reshape(block_count, tok_rows, heads_here, head_size)
    value_blocks = value_window.reshape(block_count, tok_rows, heads_here, head_size)
    bias_blocks = bias_window.astype(jnp.float32).reshape(heads_here, block_count, tok_rows)
    scores = jnp.einsum(
        "qhe,bkhe->hqbk", query_matrix_rows, key_blocks, preferred_element_type=jnp.float32
    )
    scores = scores * head_size ** (-0.5) + bias_blocks[:, None, :, :]
    block_ids = lax.broadcasted_iota(jnp.int32, scores.shape, 2)
    valid = block_ids < valid_count
    keep_log = jnp.where(valid, jax.nn.log_sigmoid(-scores), 0.0)
    later_sum = jnp.einsum(
        "hqbj,jk->hqbk", keep_log, later_matrix(tok_rows), precision=lax.Precision.HIGHEST
    )
    weights = jnp.where(valid, jnp.exp(jax.nn.log_sigmoid(scores) + later_sum), 0.0)
    block_out = jnp.einsum(
        "hqbk,bkhe->bqhe",
        weights.astype(jnp.bfloat16),
        value_blocks,
        preferred_element_type=jnp.float32,
    )
    totals = jnp.sum(keep_log, axis=3)
    after = jnp.einsum(
        "hqj,jb->hqb", totals, later_matrix(block_count), precision=lax.Precision.HIGHEST
    )
    factor = jnp.transpose(jnp.exp(after), (2, 1, 0))[:, :, :, None]
    return (jnp.sum(factor * block_out, axis=0), jnp.sum(totals, axis=2))


def combine(attended_sum, carried, block_out, block_keep):
    factor = jnp.exp(carried).T[:, :, None]
    return (attended_sum + factor * block_out, carried + block_keep)


def on_device(
    tokens,
    norm_gain,
    w_query,
    w_key,
    w_value,
    key_bias,
    w_glu_value,
    w_glu_gate,
    conv_weight,
    conv_bias,
    ln_gain,
    w_out_att,
    w_out_conv,
):
    tok_rows = tokens.shape[0]
    tp_count = lax.axis_size("tp")
    tp_index = lax.axis_index("tp")
    sp_index = lax.axis_index("sp")
    squares = jnp.sum(jnp.square(tokens.astype(jnp.float32)), axis=1)
    row_scale = lax.rsqrt(lax.psum(squares, "tp") / D + epsilon)
    matrices = (w_query, w_key, w_value, w_glu_value, w_glu_gate)
    gain_piece = norm_gain.astype(jnp.float32)
    normed = (
        lax.all_gather(tokens, "tp", axis=1, tiled=True).astype(jnp.float32)
        * row_scale[:, None]
        * gain_piece
    ).astype(jnp.bfloat16)
    projected = tuple(
        (jnp.dot(normed, matrix, preferred_element_type=jnp.float32) for matrix in matrices)
    )
    heads_here = w_query.shape[1] // HEAD
    query_matrix_rows = projected[0].astype(jnp.bfloat16).reshape(tok_rows, heads_here, HEAD)
    key_rows = projected[1].astype(jnp.bfloat16).reshape(tok_rows, heads_here, HEAD)
    value_rows = projected[2].astype(jnp.bfloat16).reshape(tok_rows, heads_here, HEAD)
    glu_value = rounded(projected[3])
    glu_gate = rounded(projected[4])
    attended_sum, carried = block_terms(query_matrix_rows, key_rows, value_rows, key_bias)
    every_key, every_value, every_bias = (
        lax.all_gather(key_rows, "sp", axis=0, tiled=True),
        lax.all_gather(value_rows, "sp", axis=0, tiled=True),
        lax.all_gather(key_bias, "sp", axis=1, tiled=True),
    )
    window_out, window_keep = window_terms(
        query_matrix_rows, every_key, every_value, every_bias, sp_index
    )
    attended_sum, carried = combine(attended_sum, carried, window_out, window_keep)
    attended = attended_sum.astype(jnp.bfloat16).reshape(tok_rows, heads_here * HEAD)
    weight_log = jnp.log(-jnp.expm1(carried))
    channels_here = w_glu_value.shape[1]
    channel_start = tp_index * channels_here
    taps_here = lax.dynamic_slice_in_dim(conv_weight, channel_start, channels_here, 1)
    bias_here = lax.dynamic_slice_in_dim(conv_bias, channel_start, channels_here, 0).astype(
        jnp.float32
    )
    gain_here = lax.dynamic_slice_in_dim(ln_gain, channel_start, channels_here, 0).astype(
        jnp.float32
    )
    gated = (glu_value * jax.nn.sigmoid(glu_gate)).astype(jnp.bfloat16)
    rim_width = conv_weight.shape[0] - 1
    rim_rows = from_behind(gated[tok_rows - rim_width :], "sp", 1)
    extended = jnp.concatenate([rim_rows, gated], axis=0)
    convolved = lax.conv_general_dilated(
        extended[None],
        taps_here[:, None, :],
        (1,),
        [(0, 0)],
        dimension_numbers=("NWC", "WIO", "NWC"),
        feature_group_count=channels_here,
        preferred_element_type=jnp.float32,
    )[0]
    convolved = convolved + bias_here[None, :]
    channel_mean = lax.psum(jnp.sum(convolved, axis=1), "tp") / CF_WIDTH
    centered = convolved - channel_mean[:, None]
    channel_var = lax.psum(jnp.sum(centered * centered, axis=1), "tp") / CF_WIDTH
    conv_out = jax.nn.silu(centered * lax.rsqrt(channel_var + epsilon)[:, None] * gain_here).astype(
        jnp.bfloat16
    )
    att_width = attended.shape[1]
    att_weight = lax.dynamic_slice_in_dim(w_out_att, tp_index * att_width, att_width, 0)
    conv_rows_weight = lax.dynamic_slice_in_dim(w_out_conv, channel_start, channels_here, 0)
    first = jnp.dot(attended, att_weight, preferred_element_type=jnp.float32)
    second = jnp.dot(
        lax.slice_in_dim(conv_out, 0, tok_rows // tp_count * lax.axis_size("tp"), axis=0),
        conv_rows_weight,
        preferred_element_type=jnp.float32,
    )
    mixed = lax.psum_scatter(first + second, "tp", scatter_dimension=0, tiled=True).astype(
        jnp.bfloat16
    )
    return (mixed, weight_log)


def solution(mesh):
    in_specs = (
        P("sp", "tp"),
        P(),
        P(None, "tp"),
        P(None, "tp"),
        P(None, "tp"),
        P("tp", "sp"),
        P(None, "tp"),
        P(None, "tp"),
        P(),
        P(),
        P(),
        P(),
        P(),
    )
    out_specs = (P(("sp", "tp"), None), P("tp", "sp"))
    return jax.shard_map(
        on_device, mesh=mesh, in_specs=in_specs, out_specs=out_specs, check_vma=False
    )
```

profile of v0, /device:TPU:0, one launch (start us, length us, event | category | flops | bytes accessed | tf_op | source)
XLA Modules:
  0.0 181.4 jit_solution(2660870203256576240)
XLA Ops:
  7.2 0.0 copy-start
  7.2 0.0 all-gather.4.cloned.1.call-start
  7.2 0.7 all-gather.4.cloned.1.call-update
  7.9 0.0 all-gather.6.cloned.1.call-start
  8.0 0.7 convert_element_type.66
  8.7 1.2 multiply_reduce_fusion
  9.8 8.4 %psum.21 = f32[384]{0:T(512)S(1)} all-reduce(f32[384]{0:T(512)S(1)} %multiply_reduce_fusion), channel_id=1, replica_groups=mesh['sp'=8,'tp'=4] {'tp'}, use_global_device_ids=true, to_apply=%region_1.0 | all-reduce | flops 384 | bytes 3072 | tf_op jit(solution)/shard_map/psum | solution.py:106
  18.2 13.8 %all-gather.4.cloned.1.call-done = bf16[384,2048]{1,0:T(8,128)(2,1)} async-done(((bf16[384,512]{1,0:T(8,128)(2,1)}), bf16[384,2048]{1,0:T(8,128)(2,1)}) %all-gather.4.cloned.1.call-update) | async-done | bytes 1572880 | tf_op jit(solution)/shard_map/all_gather | solution.py:110
  32.0 3.1 %convolution_convert_fusion.2 = bf16[384,256]{0,1:T(8,128)(2,1)} fusion(bf16[2048,256]{1,0:T(8,128)(2,1)S(1)} %copy-done, bf16[384,2048]{1,0:T(8,128)(2,1)} %all-gather.4.cloned.1.call-done, f32[2048]{0:T(1024)S(1)} %convert_element_type.66, f32[384]{0:T(512)S(1)} %add_rsqrt_fusion.1), kind=kOutput, calls=%fused_computation.35 | convolution fusion | flops 405897216 | bytes 2827776 | tf_op jit(solution)/shard_map/dot_general | solution.py:115
  35.0 0.0 all-gather.6.cloned.1.call-update
  35.0 0.0 all-gather.8.cloned.1.call-start
  35.1 26.3 %all_gather.14 = bf16[2,3072]{1,0:T(2,128)(2,1)S(1)} all-gather(bf16[2,384]{1,0:T(2,128)(2,1)S(1)} %copy-done.3), channel_id=1, replica_groups=mesh['sp'=8,'tp'=4] {'sp'}, dimensions={1}, use_global_device_ids=true | all-gather | bytes 13824 | tf_op jit(solution)/shard_map/all_gather | solution.py:127
  61.4 0.8 dynamic-slice_convert_fusion.1
  62.3 0.8 dynamic-slice_convert_fusion
  63.0 0.7 dynamic-slice_bitcast_fusion
  63.7 1.9 %convolution_convert_fusion.1 = bf16[384,256]{1,0:T(8,128)(2,1)S(1)} fusion(bf16[2048,256]{1,0:T(8,128)(2,1)} %param.19, bf16[384,2048]{1,0:T(8,128)(2,1)S(1)} %copy-done.4, f32[2048]{0:T(1024)S(1)} %convert_element_type.66, f32[384]{0:T(512)S(1)} %add_rsqrt_fusion.1), kind=kOutput, calls=%fused_computation.34 | convolution fusion | flops 405897216 | bytes 2827776 | tf_op jit(solution)/shard_map/dot_general | solution.py:115
  65.6 0.6 convolution_convert_fusion
  66.3 0.1 multiply_convert_fusion.2
  66.4 3.4 %collective-permute-start = (bf16[30,256]{1,0:T(8,128)(2,1)S(1)}, bf16[30,256]{1,0:T(8,128)(2,1)S(1)}, u32[]{:S(2)}, u32[]{:S(2)}) collective-permute-start(bf16[30,256]{1,0:T(8,128)(2,1)S(1)} %slice.6), channel_id=1, source_target_pairs={{0,4},{4,8},{8,12},{12,16},{16,20},{20,24},{24,28},{1,5},{5,9},{9,... | collective-permute-start | bytes 46088 | tf_op jit(solution)/shard_map/ppermute | solution.py:15
  69.8 0.9 convolution_convert_fusion.3
  70.7 0.4 fusion.39
  71.2 0.9 convolution_convert_fusion.4
  72.1 2.7 %fusion.15 = bf16[2,384,384]{1,2,0:T(8,128)(2,1)} fusion(f32[2,384,384]{1,2,0:T(8,128)S(1)} %get-tuple-element.7, u8[384,384]{0,1:T(8,128)(4,1)S(1)} %get-tuple-element.6), kind=kOutput, calls=%fused_computation.24 | convolution fusion | flops 1366179840 | bytes 1916928 | tf_op jit(solution)/shard_map/hqj,jk->hqk/dot_general | solution.py:39
  74.8 0.6 fusion.23
  75.3 0.8 copy.31
  76.2 0.0 all-gather.8.cloned.1.call-update
  76.2 0.0 reduce-scatter.2.cloned.1.call-start
  76.2 0.1 maximum_bitcast_fusion
  76.5 1.0 convolution_select_fusion
  77.4 0.1 copy.37
  77.6 0.1 fusion.38
  77.8 6.0 %psum.22 = f32[384]{0:T(512)S(1)} all-reduce(f32[384]{0:T(512)S(1)} %fusion.38), channel_id=1, replica_groups=mesh['sp'=8,'tp'=4] {'tp'}, use_global_device_ids=true, to_apply=%region_6.7 | all-reduce | flops 384 | bytes 3072 | tf_op jit(solution)/shard_map/psum | solution.py:158
  83.8 0.2 multiply_reduce_fusion.1
  84.0 5.9 %psum.23 = f32[384]{0:T(512)S(1)} all-reduce(f32[384]{0:T(512)S(1)} %multiply_reduce_fusion.1), channel_id=1, replica_groups=mesh['sp'=8,'tp'=4] {'tp'}, use_global_device_ids=true, to_apply=%region_8.9 | all-reduce | flops 384 | bytes 3072 | tf_op jit(solution)/shard_map/psum | solution.py:160
  90.0 0.0 all-gather.6.cloned.1.call-done
  90.0 1.9 %copy.28 = bf16[3072,2,128]{2,0,1:T(8,128)(2,1)S(1)} copy(bf16[3072,2,128]{0,2,1:T(8,128)(2,1)} %all-gather.6.cloned.1.call-done) | data formatting | bytes 3145728 | tf_op jit(solution)/shard_map/all_gather | solution.py:125
  91.9 3.4 %fusion.8 = (u8[2,384,384]{1,2,0:T(8,128)(4,1)S(1)}, f32[2,384,8,384]{1,3,2,0:T(8,128)S(1)}) fusion(f32[2,8,384]{2,1,0:T(8,128)S(1)} %bitcast.79, bf16[384,2,128,1]{0,2,3,1:T(8,128)(2,1)S(1)} %bitcast.78, bf16[8,384,2,128]{3,1,0,2:T(8,128)(2,1)S(1)} %bitcast.71), kind=kOutput, calls=%fused_computation.17 | convolution fusion | flops 620199936 | bytes 11526144 | tf_op jit(solution)/shard_map/qhe,bkhe->hqbk/dot_general | solution.py:56
  95.3 7.6 %fusion.58 = (f32[2,384]{1,0:T(2,128)S(1)}, f32[2,384,8]{1,2,0:T(8,128)S(1)}) fusion(f32[2,8,384]{2,1,0:T(8,128)S(1)} %bitcast.80, f32[2,384,8,384]{1,3,2,0:T(8,128)S(1)} %get-tuple-element.9, u8[2,384,384]{1,2,0:T(8,128)(4,1)S(1)} %get-tuple-element.8, pred[8]{0:T(512)(128)(4,1)S(1)} %iota_compare_fusion.4), kind=kLoop, calls=%fused_computation.94 | loop fusion | flops 35382528 | bytes 9784328 | tf_op jit(solution)/shard_map/reduce_sum | solution.py:78
  102.9 0.1 fusion.19
  103.1 0.6 negate_log_fusion
  103.7 23.3 %fusion.4 = bf16[2,384,8,384]{1,3,2,0:T(8,128)(2,1)} fusion(f32[2,384,8,384]{1,3,2,0:T(8,128)S(1)} %get-tuple-element.9, f32[2,8,384]{2,1,0:T(8,128)S(1)} %bitcast.81, pred[8]{0:T(512)(128)(4,1)S(1)} %iota_compare_fusion.4, u8[2,384,384]{1,2,0:T(8,128)(4,1)S(1)} %get-tuple-element.8), kind=kOutput, calls=%fused_computation.5 | convolution fusion | flops 10933125120 | bytes 14475272 | tf_op jit(solution)/shard_map/hqbj,jk->hqbk/dot_general | solution.py:63
  127.0 4.1 %fusion.7 = f32[384,2,128]{0,2,1:T(8,128)S(1)} fusion(bf16[2,384,8,384]{1,3,2,0:T(8,128)(2,1)} %fusion.4, bf16[8,384,2,128]{3,1,0,2:T(8,128)(2,1)} %bitcast.83, f32[8,384,2]{1,2,0:T(2,128)S(1)} %copy.30), kind=kOutput, calls=%fused_computation.14 | convolution fusion | flops 605454336 | bytes 6709248 | tf_op jit(solution)/shard_map/hqbk,bkhe->bqhe/dot_general | solution.py:67
  131.1 0.3 fusion.18
  131.4 1.8 %fusion.21 = f32[384,2048]{1,0:T(8,128)S(1)} fusion(bf16[384,256]{0,1:T(8,128)(2,1)S(1)} %bitcast.72, bf16[1024,2048]{1,0:T(8,128)(2,1)} %param.24, s32[]{:T(128)S(6)} %select_n.45), kind=kOutput, calls=%fused_computation.42 | convolution fusion | flops 402653184 | bytes 4390916 | tf_op jit(solution)/shard_map/dot_general | solution.py:167
  133.3 3.6 %convolution_add_fusion = f32[384,2048]{1,0:T(8,128)} fusion(f32[384,2048]{1,0:T(8,128)S(1)} %fusion.21, bf16[1024,2048]{1,0:T(8,128)(2,1)} %param.25, s32[]{:T(128)S(6)} %select_n.45, f32[1,416,256]{2,1,0:T(8,128)S(1)} %reshape.44, f32[256]{0:T(256)S(1)} %dynamic-slice_convert_fusion, f32[384]{0:T(512)S(1)} %add_rsqrt_fusion, ...), kind=kOutput, calls=%fused_computation.16 | convolution fusion | flops 404324352 | bytes 7739396 | tf_op jit(solution)/shard_map/dot_general | solution.py:168
  136.9 0.0 reduce-scatter.2.cloned.1.call-update
  136.9 36.1 %reduce-scatter.2.cloned.1.call-done = f32[96,2048]{1,0:T(8,128)} async-done(((f32[384,2048]{1,0:T(8,128)}), f32[96,2048]{1,0:T(8,128)}) %reduce-scatter.2.cloned.1.call-update) | async-done | bytes 786448 | tf_op jit(solution)/shard_map/reduce_scatter | solution.py:173
  173.0 1.9 %convert_element_type.83 = bf16[96,2048]{1,0:T(8,128)(2,1)} convert(f32[96,2048]{1,0:T(8,128)} %reduce-scatter.2.cloned.1.call-done) | non-fusion elementwise | flops 196608 | bytes 1179648 | tf_op jit(solution)/shard_map/convert_element_type | solution.py:173
  (32 shorter events, 0.3 us)
Async XLA Ops:
  7.2 24.8 %copy-start = (bf16[2048,256]{1,0:T(8,128)(2,1)S(1)}, bf16[2048,256]{1,0:T(8,128)(2,1)}, u32[]{:S(2)}) copy-start(bf16[2048,256]{1,0:T(8,128)(2,1)} %param.16) | copy-start | bytes 3145732
  7.2 27.9 %copy-start.3 = (bf16[2,384]{1,0:T(2,128)(2,1)S(1)}, bf16[2,384]{1,0:T(2,128)(2,1)}, u32[]{:S(2)}) copy-start(bf16[2,384]{1,0:T(2,128)(2,1)} %param.18) | copy-start | bytes 4612
  7.2 24.8 %all-gather.4.cloned.1.call-start = ((), (), s32[]{:S(2)}) async-start(), calls=%async_computation.1 | async-start | bytes 1966080 | tf_op jit(solution)/shard_map/all_gather | solution.py:110
  7.9 82.0 %all-gather.6.cloned.1.call-start = ((), (), s32[]{:S(2)}) async-start(), calls=%async_computation.2 | async-start | bytes 1769472 | tf_op jit(solution)/shard_map/all_gather | solution.py:125
  31.9 31.8 %copy-start.4 = (bf16[384,2048]{1,0:T(8,128)(2,1)S(1)}, bf16[384,2048]{1,0:T(8,128)(2,1)}, u32[]{:S(2)}) copy-start(bf16[384,2048]{1,0:T(8,128)(2,1)} %all-gather.4.cloned.1.call-done) | copy-start | bytes 4718596
  35.0 91.9 %all-gather.8.cloned.1.call-start = ((), (), s32[]{:S(2)}) async-start(), calls=%async_computation.3 | async-start | bytes 1769472 | tf_op jit(solution)/shard_map/all_gather | solution.py:126
  61.4 4.2 %copy-start.5 = (bf16[2048,256]{1,0:T(8,128)(2,1)S(1)}, bf16[2048,256]{1,0:T(8,128)(2,1)}, u32[]{:S(2)}) copy-start(bf16[2048,256]{1,0:T(8,128)(2,1)} %param.20) | copy-start | bytes 3145732
  65.6 4.2 %copy-start.6 = (bf16[2048,256]{1,0:T(8,128)(2,1)S(1)}, bf16[2048,256]{1,0:T(8,128)(2,1)}, u32[]{:S(2)}) copy-start(bf16[2048,256]{1,0:T(8,128)(2,1)} %param.15) | copy-start | bytes 3145732
  66.3 4.5 %copy-start.1 = (bf16[384,256]{0,1:T(8,128)(2,1)S(1)}, bf16[384,256]{0,1:T(8,128)(2,1)}, u32[]{:S(2)}) copy-start(bf16[384,256]{0,1:T(8,128)(2,1)} %convolution_convert_fusion.2) | copy-start | bytes 589828
  66.3 4.9 %copy-start.7 = (bf16[2048,256]{1,0:T(8,128)(2,1)S(1)}, bf16[2048,256]{1,0:T(8,128)(2,1)}, u32[]{:S(2)}) copy-start(bf16[2048,256]{1,0:T(8,128)(2,1)} %param.17) | copy-start | bytes 3145732
  66.4 9.8 %collective-permute-start = (bf16[30,256]{1,0:T(8,128)(2,1)S(1)}, bf16[30,256]{1,0:T(8,128)(2,1)S(1)}, u32[]{:S(2)}, u32[]{:S(2)}) collective-permute-start(bf16[30,256]{1,0:T(8,128)(2,1)S(1)} %slice.6), channel_id=1, source_target_pairs={{0,4},{4,8},{8,12},{12,16},{16,20},{20,24},{24,28},{1,5},{5,9},{9,... | collective-permute-start | bytes 46088 | tf_op jit(solution)/shard_map/ppermute | solution.py:15
  74.8 1.7 copy-start.8
  76.2 96.8 %reduce-scatter.2.cloned.1.call-start = ((), (), s32[]{:S(2)}) async-start(), calls=%async_computation.4 | async-start | bytes 3932160 | tf_op jit(solution)/shard_map/reduce_scatter | solution.py:173
  127.0 4.2 %copy-start.2 = (bf16[2,384,384]{1,2,0:T(8,128)(2,1)S(1)}, bf16[2,384,384]{1,2,0:T(8,128)(2,1)}, u32[]{:S(2)}) copy-start(bf16[2,384,384]{1,2,0:T(8,128)(2,1)} %fusion.15) | copy-start | bytes 1769476
Sparse Core Ops, SparseCore 0:
  9.6 22.3 all-gather.3
  35.2 44.7 all-gather.5
  82.2 42.4 all-gather.7
  137.0 35.9 reduce-scatter.1
where the time goes:
time: 182 us; the launch traced here: 181 us
  waiting for transfers between devices  50.6 us (28%)
  matrix products  48.1 us (26%)
  blocking collectives  46.5 us (26%)
  other arithmetic  14.7 us (8%)
  between operations  14.1 us (8%)
  local copies, waits for them, and re-layouts  3.85 us (2%)
  starting transfers between devices  3.56 us (2%)
    reduce_scatter x1, waiting for transfers between devices, on_device(): lax.psum_scatter(first + second, 'tp', scatter_dimension=0, tiled=True)  36.1 us
    all_gather x1, blocking collectives, on_device(): lax.all_gather(key_bias, 'sp', axis=1, tiled=True)  26.3 us
    dot_general x1, matrix products, window_terms(): jnp.einsum('hqbj,jk->hqbk', keep_log, later_matrix(tok_rows), precision=l...  23.3 us
    all_gather x1, waiting for transfers between devices, on_device(): lax.all_gather(tokens, 'tp', axis=1, tiled=True).astype(jnp.float32)  13.8 us
    psum x1, blocking collectives, on_device(): row_scale = lax.rsqrt(lax.psum(squares, 'tp') / D + epsilon)  8.37 us
    reduce_sum x1, other arithmetic, window_terms(): return (jnp.sum(factor * block_out, axis=0), jnp.sum(totals, axis=2))  7.62 us
    dot_general x5, matrix products, on_device(): jnp.dot(normed, matrix, preferred_element_type=jnp.float32)  7.31 us
    psum x1, blocking collectives, on_device(): channel_mean = lax.psum(jnp.sum(convolved, axis=1), 'tp') / CF_WIDTH  5.98 us
  transfers between devices with their start and end apart: 5, of which 2 were waited for; matrix products, arithmetic and copies ran while one was open for 29% of the time, Pallas kernels for 0%

commit v1 on v0

--- a/solution.py
+++ b/solution.py
@@ -124,7 +124,7 @@
     every_key, every_value, every_bias = (
         lax.all_gather(key_rows, "sp", axis=0, tiled=True),
         lax.all_gather(value_rows, "sp", axis=0, tiled=True),
-        lax.all_gather(key_bias, "sp", axis=1, tiled=True),
+        jnp.concatenate(lax.all_gather(key_bias, "sp"), axis=1),
     )
     window_out, window_keep = window_terms(
         query_matrix_rows, every_key, every_value, every_bias, sp_index

time: 182 us -> 191 us (1.049)
  waiting for transfers between devices: 50.6 us -> 59.4 us
    all_gather x1, waiting for transfers between devices: 0.01 us -> 14.7 us  [on_device(): lax.all_gather(key_rows, 'sp', axis=0, tiled=True)]
    all_gather x1, waiting for transfers between devices: 13.8 us -> 0.02 us  [on_device(): lax.all_gather(tokens, 'tp', axis=1, tiled=True).astype(jnp.float32)]
    all_gather x1, waiting for transfers between devices: 0.01 us -> 7.62 us  [on_device(): lax.all_gather(value_rows, 'sp', axis=0, tiled=True)]
  transfers between devices with their start and end apart: 5 -> 5, of which waited for: 2 -> 3; matrix products, arithmetic and copies ran while one was open for 29% -> 27% of each run, Pallas kernels for 0% -> 0%
where the time goes in v1:
time: 191 us
  waiting for transfers between devices  59.4 us (31%)
  matrix products  48.1 us (25%)
  blocking collectives  47 us (25%)
  other arithmetic  14.7 us (8%)
  between operations  14.1 us (7%)
  local copies, waits for them, and re-layouts  3.85 us (2%)
  starting transfers between devices  3.57 us (2%)
    reduce_scatter x1, waiting for transfers between devices, on_device(): lax.psum_scatter(first + second, 'tp', scatter_dimension=0, tiled=True)  36.4 us
    all_gather x1, blocking collectives, on_device(): lax.all_gather(key_bias, 'sp')  26.5 us
    dot_general x1, matrix products, window_terms(): jnp.einsum('hqbj,jk->hqbk', keep_log, later_matrix(tok_rows), precision=l...  23.3 us
    all_gather x1, waiting for transfers between devices, on_device(): lax.all_gather(key_rows, 'sp', axis=0, tiled=True)  14.7 us
    psum x1, blocking collectives, on_device(): row_scale = lax.rsqrt(lax.psum(squares, 'tp') / D + epsilon)  8.37 us
    reduce_sum x1, other arithmetic, window_terms(): return (jnp.sum(factor * block_out, axis=0), jnp.sum(totals, axis=2))  7.62 us
    all_gather x1, waiting for transfers between devices, on_device(): lax.all_gather(value_rows, 'sp', axis=0, tiled=True)  7.62 us
    dot_general x5, matrix products, on_device(): jnp.dot(normed, matrix, preferred_element_type=jnp.float32)  7.33 us
  transfers between devices with their start and end apart: 5, of which 3 were waited for; matrix products, arithmetic and copies ran while one was open for 27% of the time, Pallas kernels for 0%

profile of v1, /device:TPU:0, one launch (start us, length us, event | category | flops | bytes accessed | tf_op | source)
XLA Modules:
  0.0 190.7 jit_solution(14957023183957187456)
XLA Ops:
  7.2 0.0 all-gather.6.cloned.1.call-start
  7.2 0.7 all-gather.6.cloned.1.call-update
  7.9 0.0 all-gather.8.cloned.1.call-start
  8.0 0.7 convert_element_type.73
  8.7 1.2 multiply_reduce_fusion
  9.8 8.4 %psum.21 = f32[384]{0:T(512)S(1)} all-reduce(f32[384]{0:T(512)S(1)} %multiply_reduce_fusion), channel_id=1, replica_groups=mesh['sp'=8,'tp'=4] {'tp'}, use_global_device_ids=true, to_apply=%region_1.0 | all-reduce | flops 384 | bytes 3072 | tf_op jit(solution)/shard_map/psum | solution.py:106
  18.2 26.5 %all-gather.1 = bf16[8,2,384]{2,1,0:T(2,128)(2,1)S(1)} all-gather(bf16[1,2,384]{2,1,0:T(2,128)(2,1)} %bitcast.77), channel_id=2, replica_groups=mesh['sp'=8,'tp'=4] {'sp'}, dimensions={0}, use_global_device_ids=true | all-gather | bytes 13824 | tf_op jit(solution)/shard_map/all_gather | solution.py:127
  44.7 0.0 all-gather.6.cloned.1.call-done
  44.8 3.1 %convolution_convert_fusion.2 = bf16[384,256]{0,1:T(8,128)(2,1)} fusion(bf16[2048,256]{1,0:T(8,128)(2,1)S(1)} %copy-done, bf16[384,2048]{1,0:T(8,128)(2,1)} %all-gather.6.cloned.1.call-done, f32[2048]{0:T(1024)S(1)} %convert_element_type.73, f32[384]{0:T(512)S(1)} %add_rsqrt_fusion.1), kind=kOutput, calls=%fused_computation.35 | convolution fusion | flops 405897216 | bytes 2827776 | tf_op jit(solution)/shard_map/dot_general | solution.py:115
  47.8 0.0 all-gather.8.cloned.1.call-update
  47.8 0.0 all-gather.10.cloned.1.call-start
  48.0 0.8 dynamic-slice_convert_fusion.1
  48.8 0.8 dynamic-slice_convert_fusion
  49.6 0.7 dynamic-slice_bitcast_fusion
  50.3 1.9 convolution_convert_fusion.1
  52.2 0.6 convolution_convert_fusion
  52.8 0.1 multiply_convert_fusion.2
  53.0 3.4 %collective-permute-start = (bf16[30,256]{1,0:T(8,128)(2,1)S(1)}, bf16[30,256]{1,0:T(8,128)(2,1)S(1)}, u32[]{:S(2)}, u32[]{:S(2)}) collective-permute-start(bf16[30,256]{1,0:T(8,128)(2,1)S(1)} %slice.6), channel_id=1, source_target_pairs={{0,4},{4,8},{8,12},{12,16},{16,20},{20,24},{24,28},{1,5},{5,9},{9,... | collective-permute-start | bytes 46088 | tf_op jit(solution)/shard_map/ppermute | solution.py:15
  56.4 0.9 convolution_convert_fusion.3
  57.3 0.4 fusion.39
  57.8 0.9 convolution_convert_fusion.4
  58.6 2.7 %fusion.15 = bf16[2,384,384]{1,2,0:T(8,128)(2,1)} fusion(f32[2,384,384]{1,2,0:T(8,128)S(1)} %get-tuple-element.7, u8[384,384]{0,1:T(8,128)(4,1)S(1)} %get-tuple-element.6), kind=kOutput, calls=%fused_computation.24 | convolution fusion | flops 1366179840 | bytes 1916928 | tf_op jit(solution)/shard_map/hqj,jk->hqk/dot_general | solution.py:39
  61.3 0.6 fusion.23
  61.9 0.8 copy.49
  62.7 0.0 all-gather.10.cloned.1.call-update
  62.7 0.0 reduce-scatter.2.cloned.1.call-start
  62.8 0.1 maximum_bitcast_fusion
  63.0 1.0 convolution_select_fusion
  64.0 0.1 copy.57
  64.2 0.1 fusion.38
  64.3 6.1 %psum.22 = f32[384]{0:T(512)S(1)} all-reduce(f32[384]{0:T(512)S(1)} %fusion.38), channel_id=1, replica_groups=mesh['sp'=8,'tp'=4] {'tp'}, use_global_device_ids=true, to_apply=%region_6.7 | all-reduce | flops 384 | bytes 3072 | tf_op jit(solution)/shard_map/psum | solution.py:158
  70.4 0.2 multiply_reduce_fusion.1
  70.6 6.1 %psum.23 = f32[384]{0:T(512)S(1)} all-reduce(f32[384]{0:T(512)S(1)} %multiply_reduce_fusion.1), channel_id=1, replica_groups=mesh['sp'=8,'tp'=4] {'tp'}, use_global_device_ids=true, to_apply=%region_8.9 | all-reduce | flops 384 | bytes 3072 | tf_op jit(solution)/shard_map/psum | solution.py:160
  76.7 14.7 %all-gather.8.cloned.1.call-done = bf16[3072,2,128]{0,2,1:T(8,128)(2,1)} async-done(((bf16[384,2,128]{0,2,1:T(8,128)(2,1)}), bf16[3072,2,128]{0,2,1:T(8,128)(2,1)}) %all-gather.8.cloned.1.call-update) | async-done | bytes 1572880 | tf_op jit(solution)/shard_map/all_gather | solution.py:125
  91.3 1.9 copy.45
  93.3 3.4 %fusion.8 = (u8[2,384,384]{1,2,0:T(8,128)(4,1)S(1)}, f32[2,384,8,384]{1,3,2,0:T(8,128)S(1)}) fusion(f32[2,8,384]{2,1,0:T(8,128)S(1)} %copy.47, bf16[384,2,128,1]{0,2,3,1:T(8,128)(2,1)S(1)} %bitcast.76, bf16[8,384,2,128]{3,1,0,2:T(8,128)(2,1)S(1)} %bitcast.69), kind=kOutput, calls=%fused_computation.17 | convolution fusion | flops 620199936 | bytes 11526144 | tf_op jit(solution)/shard_map/qhe,bkhe->hqbk/dot_general | solution.py:56
  96.7 7.6 %fusion.58 = (f32[2,384]{1,0:T(2,128)S(1)}, f32[2,384,8]{1,2,0:T(8,128)S(1)}) fusion(f32[2,8,384]{2,1,0:T(8,128)S(1)} %copy.47, f32[2,384,8,384]{1,3,2,0:T(8,128)S(1)} %get-tuple-element.9, u8[2,384,384]{1,2,0:T(8,128)(4,1)S(1)} %get-tuple-element.8, pred[8]{0:T(512)(128)(4,1)S(1)} %iota_compare_fusion.4), kind=kLoop, calls=%fused_computation.94 | loop fusion | flops 35382528 | bytes 9784328 | tf_op jit(solution)/shard_map/reduce_sum | solution.py:78
  104.3 0.1 fusion.19
  104.5 0.6 negate_log_fusion
  105.1 23.3 %fusion.4 = bf16[2,384,8,384]{1,3,2,0:T(8,128)(2,1)} fusion(f32[2,384,8,384]{1,3,2,0:T(8,128)S(1)} %get-tuple-element.9, f32[2,8,384]{2,1,0:T(8,128)S(1)} %copy.47, pred[8]{0:T(512)(128)(4,1)S(1)} %iota_compare_fusion.4, u8[2,384,384]{1,2,0:T(8,128)(4,1)S(1)} %get-tuple-element.8), kind=kOutput, calls=%fused_computation.5 | convolution fusion | flops 10933125120 | bytes 14475272 | tf_op jit(solution)/shard_map/hqbj,jk->hqbk/dot_general | solution.py:63
  128.3 7.6 %all-gather.10.cloned.1.call-done = bf16[3072,2,128]{2,0,1:T(8,128)(2,1)} async-done(((bf16[384,2,128]{2,0,1:T(8,128)(2,1)}), bf16[3072,2,128]{2,0,1:T(8,128)(2,1)}) %all-gather.10.cloned.1.call-update) | async-done | bytes 1572880 | tf_op jit(solution)/shard_map/all_gather | solution.py:126
  136.0 4.1 %fusion.7 = f32[384,2,128]{0,2,1:T(8,128)S(1)} fusion(bf16[2,384,8,384]{1,3,2,0:T(8,128)(2,1)} %fusion.4, bf16[8,384,2,128]{3,1,0,2:T(8,128)(2,1)} %bitcast.78, f32[8,384,2]{1,2,0:T(2,128)S(1)} %copy.48), kind=kOutput, calls=%fused_computation.14 | convolution fusion | flops 605454336 | bytes 6709248 | tf_op jit(solution)/shard_map/hqbk,bkhe->bqhe/dot_general | solution.py:67
  140.1 0.3 fusion.18
  140.4 1.8 fusion.21
  142.2 3.6 %convolution_add_fusion = f32[384,2048]{1,0:T(8,128)} fusion(f32[384,2048]{1,0:T(8,128)S(1)} %fusion.21, bf16[1024,2048]{1,0:T(8,128)(2,1)} %param.25, s32[]{:T(128)S(6)} %select_n.45, f32[1,416,256]{2,1,0:T(8,128)S(1)} %reshape.48, f32[256]{0:T(256)S(1)} %dynamic-slice_convert_fusion, f32[384]{0:T(512)S(1)} %add_rsqrt_fusion, ...), kind=kOutput, calls=%fused_computation.16 | convolution fusion | flops 404324352 | bytes 7739396 | tf_op jit(solution)/shard_map/dot_general | solution.py:168
  145.8 0.0 reduce-scatter.2.cloned.1.call-update
  145.9 36.4 %reduce-scatter.2.cloned.1.call-done = f32[96,2048]{1,0:T(8,128)} async-done(((f32[384,2048]{1,0:T(8,128)}), f32[96,2048]{1,0:T(8,128)}) %reduce-scatter.2.cloned.1.call-update) | async-done | bytes 786448 | tf_op jit(solution)/shard_map/reduce_scatter | solution.py:173
  182.3 1.9 %convert_element_type.92 = bf16[96,2048]{1,0:T(8,128)(2,1)} convert(f32[96,2048]{1,0:T(8,128)} %reduce-scatter.2.cloned.1.call-done) | non-fusion elementwise | flops 196608 | bytes 1179648 | tf_op jit(solution)/shard_map/convert_element_type | solution.py:173
  (33 shorter events, 0.3 us)
Async XLA Ops:
  7.2 37.6 %copy-start = (bf16[2048,256]{1,0:T(8,128)(2,1)S(1)}, bf16[2048,256]{1,0:T(8,128)(2,1)}, u32[]{:S(2)}) copy-start(bf16[2048,256]{1,0:T(8,128)(2,1)} %param.16) | copy-start | bytes 3145732
  7.2 40.7 %copy-start.3 = (bf16[2,384]{1,0:T(2,128)(2,1)S(1)}, bf16[2,384]{1,0:T(2,128)(2,1)}, u32[]{:S(2)}) copy-start(bf16[2,384]{1,0:T(2,128)(2,1)} %param.18) | copy-start | bytes 4612
  7.2 37.5 %all-gather.6.cloned.1.call-start = ((), (), s32[]{:S(2)}) async-start(), calls=%async_computation.1 | async-start | bytes 1966080 | tf_op jit(solution)/shard_map/all_gather | solution.py:110
  7.9 83.4 %all-gather.8.cloned.1.call-start = ((), (), s32[]{:S(2)}) async-start(), calls=%async_computation.2 | async-start | bytes 1769472 | tf_op jit(solution)/shard_map/all_gather | solution.py:125
  44.7 5.5 %copy-start.4 = (bf16[384,2048]{1,0:T(8,128)(2,1)S(1)}, bf16[384,2048]{1,0:T(8,128)(2,1)}, u32[]{:S(2)}) copy-start(bf16[384,2048]{1,0:T(8,128)(2,1)} %all-gather.6.cloned.1.call-done) | copy-start | bytes 4718596
  47.8 88.1 %all-gather.10.cloned.1.call-start = ((), (), s32[]{:S(2)}) async-start(), calls=%async_computation.3 | async-start | bytes 1769472 | tf_op jit(solution)/shard_map/all_gather | solution.py:126
  47.9 4.2 %copy-start.5 = (bf16[2048,256]{1,0:T(8,128)(2,1)S(1)}, bf16[2048,256]{1,0:T(8,128)(2,1)}, u32[]{:S(2)}) copy-start(bf16[2048,256]{1,0:T(8,128)(2,1)} %param.20) | copy-start | bytes 3145732
  52.2 4.2 %copy-start.6 = (bf16[2048,256]{1,0:T(8,128)(2,1)S(1)}, bf16[2048,256]{1,0:T(8,128)(2,1)}, u32[]{:S(2)}) copy-start(bf16[2048,256]{1,0:T(8,128)(2,1)} %param.15) | copy-start | bytes 3145732
  52.8 4.5 %copy-start.1 = (bf16[384,256]{0,1:T(8,128)(2,1)S(1)}, bf16[384,256]{0,1:T(8,128)(2,1)}, u32[]{:S(2)}) copy-start(bf16[384,256]{0,1:T(8,128)(2,1)} %convolution_convert_fusion.2) | copy-start | bytes 589828
  52.8 4.9 %copy-start.7 = (bf16[2048,256]{1,0:T(8,128)(2,1)S(1)}, bf16[2048,256]{1,0:T(8,128)(2,1)}, u32[]{:S(2)}) copy-start(bf16[2048,256]{1,0:T(8,128)(2,1)} %param.17) | copy-start | bytes 3145732
  53.0 9.8 %collective-permute-start = (bf16[30,256]{1,0:T(8,128)(2,1)S(1)}, bf16[30,256]{1,0:T(8,128)(2,1)S(1)}, u32[]{:S(2)}, u32[]{:S(2)}) collective-permute-start(bf16[30,256]{1,0:T(8,128)(2,1)S(1)} %slice.6), channel_id=1, source_target_pairs={{0,4},{4,8},{8,12},{12,16},{16,20},{20,24},{24,28},{1,5},{5,9},{9,... | collective-permute-start | bytes 46088 | tf_op jit(solution)/shard_map/ppermute | solution.py:15
  61.3 1.7 copy-start.8
  62.7 119.5 %reduce-scatter.2.cloned.1.call-start = ((), (), s32[]{:S(2)}) async-start(), calls=%async_computation.4 | async-start | bytes 3932160 | tf_op jit(solution)/shard_map/reduce_scatter | solution.py:173
  136.0 4.2 %copy-start.2 = (bf16[2,384,384]{1,2,0:T(8,128)(2,1)S(1)}, bf16[2,384,384]{1,2,0:T(8,128)(2,1)}, u32[]{:S(2)}) copy-start(bf16[2,384,384]{1,2,0:T(8,128)(2,1)} %fusion.15) | copy-start | bytes 1769476
Sparse Core Ops, SparseCore 0:
  9.6 22.3 all-gather.5
  48.0 43.3 all-gather.7
  93.5 42.3 all-gather.9
  146.0 36.2 reduce-scatter.1
